TPU v7x, 256 devices: a whole 4x4x8 slice. The times are simulated.
256 devices in a mesh: sp: 32 (over z, y), tp: 8 (over x, core).
Axes of the slice: x: 4, y: 4, z: 8, core: 2. Of those that a mesh axis runs over, the one named last changes fastest.
Arguments:
- tokens: bfloat16 [16384, 2048], P('sp', 'tp'), may hold values from -64 to 64
- conv_input: bfloat16 [2048, 1024], P(None, 'tp'), may hold values from -0.125 to 0.125
- conv_inner: bfloat16 [2048, 1024], P(None, 'tp'), may hold values from -0.125 to 0.125
- conv_outer: bfloat16 [2048, 1024], P(None, 'tp'), may hold values from -0.125 to 0.125
- conv_gate: bfloat16 [2048, 1024], P(None, 'tp'), may hold values from -0.125 to 0.125
- conv_taps: bfloat16 [3, 1024], P(None, 'tp'), may hold values from -3.5 to 3.5
- query_proj: bfloat16 [2048, 1536], P(None, 'tp'), may hold values from -8 to 8
- latent_proj: bfloat16 [2048, 256], replicated, may hold values from -1 to 1
- rope_proj: bfloat16 [2048, 32], replicated, may hold values from -0.125 to 0.125
- latent_gain: float32 [256], replicated, may hold values from 0.1 to 1.9
- key_up: bfloat16 [256, 1024], P(None, 'tp'), may hold values from -2 to 2
- value_up: bfloat16 [256, 1024], P(None, 'tp'), may hold values from -0.375 to 0.375
- attn_gate: bfloat16 [2048, 1024], P(None, 'tp'), may hold values from -0.125 to 0.125
- conv_down: bfloat16 [1024, 2048], P('tp'), may hold values from -0.1875 to 0.1875
- attn_down: bfloat16 [1024, 2048], P('tp'), may hold values from -0.75 to 0.75
Outputs:
- layer_out: bfloat16 [16384, 2048], P(('sp', 'tp'))
All inputs are finite; a program needn't handle non-finite values.
Results may differ from a plain program's by a relative error of at most 0.014.
Values may be sent and summed in bfloat16 or wider, within the bound.
A program may use at most 128 MiB of HBM per device.

v0:
```python
import jax
import jax.numpy as jnp
from jax import lax
from jax.sharding import PartitionSpec as P

NOPE = 64
ROPE = 32
VDIM = 64
GRID_W = 64


rms_eps = 1e-06
rope_theta = 10000.0


def joined_along(parts, dim):
    lengths = list(parts.shape[1:])
    lengths[dim] *= parts.shape[0]
    return jnp.moveaxis(parts, 0, dim).reshape(lengths)


def sent_to_all(value, axis):
    length = lax.axis_size(axis)
    return lax.all_to_all(
        jnp.broadcast_to(value[None], (length, *value.shape)), axis, 0, 0, tiled=True
    )


def collect(value, axis, dim):
    return joined_along(sent_to_all(value, axis), dim)


def with_halo(cells, sides, width):
    for axis, dim in sides:
        count = lax.axis_size(axis)
        ends = count - 1
        head = lax.slice_in_dim(cells, 0, width, axis=dim)
        tail = lax.slice_in_dim(cells, cells.shape[dim] - width, cells.shape[dim], axis=dim)
        cells = jnp.concatenate(
            [
                lax.ppermute(tail, axis, [(i, (i + 1) % count) for i in range(ends)]),
                cells,
                lax.ppermute(head, axis, [((i + 1) % count, i) for i in range(ends)]),
            ],
            axis=dim,
        )
    return cells


def sent_together(arrays, axis, dim, along):
    both = jnp.concatenate(arrays, axis=along)
    whole, at, finished = (lax.all_gather(both, axis, axis=dim, tiled=True), 0, [])
    for a in arrays:
        finished.append(lax.slice_in_dim(whole, at, at + a.shape[along], axis=along))
        at += a.shape[along]
    return tuple(finished)


def cut_along(value, dim, length):
    lengths = value.shape
    parts = value.reshape(*lengths[:dim], length, lengths[dim] // length, *lengths[dim + 1 :])
    return jnp.moveaxis(parts, dim, 0)


def sum_at_owner(value, axis, dim):
    parts = cut_along(value, dim, lax.axis_size(axis))
    arrived = lax.all_to_all(parts, axis, split_axis=0, concat_axis=0, tiled=True)
    return arrived.astype(jnp.float32).sum(axis=0)


def rounded(values):
    return lax.optimization_barrier(values.astype(jnp.bfloat16))


def axial_tables(positions, rope_width, grid_width):
    quarter = rope_width // 4
    frequency = rope_theta ** (-jnp.arange(quarter, dtype=jnp.float32) * 2.0 / (rope_width // 2))
    grid_row = (positions // grid_width).astype(jnp.float32)
    grid_col = (positions % grid_width).astype(jnp.float32)
    row_angle = grid_row[:, None] * frequency[None, :]
    col_angle = grid_col[:, None] * frequency[None, :]
    return (jnp.cos(row_angle), jnp.sin(row_angle), jnp.cos(col_angle), jnp.sin(col_angle))


def turn_half(vector, cos_table, sin_table):
    half_width = vector.shape[-1] // 2
    leading = vector[..., :half_width]
    trailing = vector[..., half_width:]
    return jnp.concatenate(
        [leading * cos_table - trailing * sin_table, trailing * cos_table + leading * sin_table],
        axis=-1,
    )


def axial_turn(vector, tables):
    half_width = vector.shape[-1] // 2
    return jnp.concatenate(
        [
            turn_half(vector[..., :half_width], tables[0], tables[1]),
            turn_half(vector[..., half_width:], tables[2], tables[3]),
        ],
        axis=-1,
    )


def on_device(
    tokens,
    conv_input,
    conv_inner,
    conv_outer,
    conv_gate,
    conv_taps,
    query_proj,
    latent_proj,
    rope_proj,
    latent_gain,
    key_up,
    value_up,
    attn_gate,
    conv_down,
    attn_down,
):
    tok_rows = tokens.shape[0]
    model_width = query_proj.shape[0]
    local_heads = key_up.shape[1] // NOPE
    in_weights = (
        conv_input,
        conv_inner,
        conv_outer,
        conv_gate,
        query_proj,
        latent_proj,
        rope_proj,
        attn_gate,
    )
    shard_piece = collect(tokens, "tp", 1)
    widened_piece = shard_piece.astype(jnp.float32)
    new_terms = tuple(
        (jnp.dot(shard_piece, matrix, preferred_element_type=jnp.float32) for matrix in in_weights)
    )
    projected = tuple((right_sum for right_sum in new_terms))
    squares = jnp.sum(widened_piece * widened_piece, axis=1)
    row_scale = lax.rsqrt(squares / model_width + rms_eps)[:, None]
    value_in, inner_in, outer_in, gate_in, queries, latent, rope_in, gate_attn = tuple(
        (proj_term * row_scale for proj_term in projected)
    )
    conv_product = (
        rounded(inner_in).astype(jnp.float32) * rounded(value_in).astype(jnp.float32)
    ).astype(jnp.bfloat16)
    padded = with_halo(conv_product, (("sp", 0),), 1).astype(jnp.float32)
    tap_weights = conv_taps.astype(jnp.float32)
    conv_mixed = (
        padded[:-2] * tap_weights[0] + padded[1:-1] * tap_weights[1] + padded[2:] * tap_weights[2]
    )
    conv_out = (
        jax.nn.silu(rounded(gate_in).astype(jnp.float32))
        * rounded(outer_in).astype(jnp.float32)
        * conv_mixed
    ).astype(jnp.bfloat16)
    positions = lax.axis_index("sp") * tok_rows + jnp.arange(tok_rows, dtype=jnp.int32)
    tables = axial_tables(positions, ROPE, GRID_W)
    queries = queries.reshape(tok_rows, local_heads, NOPE + ROPE)
    query_nope = queries[..., :NOPE].astype(jnp.bfloat16)
    query_rope = axial_turn(
        queries[..., NOPE:], tuple((grid_table[:, None, :] for grid_table in tables))
    ).astype(jnp.bfloat16)
    latent = (
        latent * lax.rsqrt(jnp.mean(latent * latent, axis=1, keepdims=True) + rms_eps) * latent_gain
    ).astype(jnp.bfloat16)
    key_rope = axial_turn(rope_in, tables).astype(jnp.bfloat16)
    score_scale = (NOPE + ROPE) ** (-0.5)
    initial = (
        jnp.full((tok_rows, local_heads), -jnp.inf, jnp.float32),
        jnp.zeros((tok_rows, local_heads), jnp.float32),
        jnp.zeros((tok_rows, local_heads, VDIM), jnp.float32),
    )
    latent_piece, rope_piece = sent_together((latent, key_rope), "sp", 0, 1)
    key_count = latent_piece.shape[0]
    span_rows = key_count
    while span_rows > 1024 and span_rows % 2 == 0:
        span_rows = span_rows // 2

    def one_span(state_now, span_start):
        latent_span = lax.dynamic_slice_in_dim(latent_piece, span_start, span_rows, 0)
        rope_span = lax.dynamic_slice_in_dim(rope_piece, span_start, span_rows, 0)
        key_nope = (
            jnp.dot(latent_span, key_up, preferred_element_type=jnp.float32)
            .astype(jnp.bfloat16)
            .reshape(span_rows, local_heads, NOPE)
        )
        key_values = (
            jnp.dot(latent_span, value_up, preferred_element_type=jnp.float32)
            .astype(jnp.bfloat16)
            .reshape(span_rows, local_heads, VDIM)
        )
        scores = jnp.einsum(
            "qhd,khd->qhk", query_nope, key_nope, preferred_element_type=jnp.float32
        )
        scores = (
            scores
            + jnp.einsum("qhd,kd->qhk", query_rope, rope_span, preferred_element_type=jnp.float32)
        ) * score_scale
        row_top, weight_total, weighted = state_now
        new_top = jnp.maximum(row_top, jnp.max(scores, axis=2))
        weights = jnp.exp(scores - new_top[:, :, None])
        shrink = jnp.exp(row_top - new_top)
        weight_total = weight_total * shrink + jnp.sum(weights, axis=2)
        weighted = weighted * shrink[:, :, None] + jnp.einsum(
            "qhk,khd->qhd",
            weights.astype(jnp.bfloat16),
            key_values,
            preferred_element_type=jnp.float32,
        )
        return ((new_top, weight_total, weighted), None)

    span_starts = jnp.arange(key_count // span_rows, dtype=jnp.int32) * span_rows
    gathered_state = lax.scan(one_span, initial, span_starts)[0]
    attended = (gathered_state[2] / gathered_state[1][:, :, None]).reshape(
        tok_rows, local_heads * VDIM
    )
    attn_out = (jax.nn.silu(rounded(gate_attn).astype(jnp.float32)) * attended).astype(jnp.bfloat16)
    summed = sum_at_owner(
        (
            jnp.dot(conv_out, conv_down, preferred_element_type=jnp.float32)
            + jnp.dot(attn_out, attn_down, preferred_element_type=jnp.float32)
        ).astype(jnp.bfloat16),
        "tp",
        0,
    )
    return summed.astype(jnp.bfloat16)


def solution(mesh):
    placed = (
        P("sp", "tp"),
        P(None, "tp"),
        P(None, "tp"),
        P(None, "tp"),
        P(None, "tp"),
        P(None, "tp"),
        P(None, "tp"),
        P(),
        P(),
        P(),
        P(None, "tp"),
        P(None, "tp"),
        P(None, "tp"),
        P("tp", None),
        P("tp", None),
    )
    return jax.shard_map(
        on_device, mesh=mesh, in_specs=placed, out_specs=P(("sp", "tp"), None), check_vma=False
    )
```

profile of v0, /device:TPU:1, one launch (start us, length us, event | category | flops | bytes accessed | tf_op | source)
XLA Modules:
  0.0 343.3 jit_solution(7264327126652506864)
XLA Ops:
  7.7 1.5 broadcast_in_dim.8
  9.2 6.7 %all-to-all-start = ((bf16[8,512,256]{1,2,0:T(8,128)(2,1)}), bf16[8,512,256]{1,2,0:T(8,128)(2,1)S(1)}, u32[]{:S(2)}, u32[]{:S(2)}) async-start(bf16[8,512,256]{1,2,0:T(8,128)(2,1)} %broadcast_in_dim.8), calls=%async_computation | async-start | bytes 4194304 | tf_op jit(solution)/shard_map/all_to_all | solution.py:24
  16.0 26.2 %all-to-all-done = bf16[8,512,256]{1,2,0:T(8,128)(2,1)S(1)} async-done(((bf16[8,512,256]{1,2,0:T(8,128)(2,1)}), bf16[8,512,256]{1,2,0:T(8,128)(2,1)S(1)}, u32[]{:S(2)}, u32[]{:S(2)}) %all-to-all-start) | async-done | bytes 2097184 | tf_op jit(solution)/shard_map/all_to_all | solution.py:24
  48.1 1.8 fusion.23
  50.7 2.4 collective-permute-start
  58.1 2.7 fusion.40
  60.8 91.8 %all-gather.2.cloned.1.call-done = bf16[16384,288]{0,1:T(8,128)(2,1)} async-done(((bf16[512,288]{0,1:T(8,128)(2,1)}), bf16[16384,288]{0,1:T(8,128)(2,1)}) %all-gather.2.cloned.1.call-update) | async-done | bytes 9437200 | tf_op jit(solution)/shard_map/all_gather | solution.py:52
  152.6 7.7 %slice.101 = bf16[16384,256]{0,1:T(8,128)(2,1)} slice(bf16[16384,288]{0,1:T(8,128)(2,1)} %all-gather.2.cloned.1.call-done), slice={[0:16384], [0:256]} | slice | bytes 16777216 | tf_op jit(solution)/shard_map/slice | solution.py:54
  160.3 137.5 %while.15 = (s32[]{:T(128)}, f32[512,2]{0,1:T(2,128)S(1)}, f32[512,2]{0,1:T(2,128)S(1)}, f32[512,2,64]{0,2,1:T(8,128)S(1)}, s32[16]{0:T(128)S(1)}, /*index=5*/bf...) while((s32[]{:T(128)}, f32[512,2]{0,1:T(2,128)S(1)}, ...), condition=%wide.region_5.6_spmd.clone, body=%wide.region_2.5_spmd.clone.sunk | while | flops 477565952 | bytes 24051920 | solution.py:217
  164.3 1.5 convolution_convert_fusion.4
  172.9 1.5 convolution_convert_fusion.4
  181.5 1.5 convolution_convert_fusion.4
  188.7 1.5 convolution_convert_fusion.5
  190.1 1.5 convolution_convert_fusion.4
  197.2 1.5 convolution_convert_fusion.5
  198.7 1.5 convolution_convert_fusion.4
  207.3 1.5 convolution_convert_fusion.4
  215.9 1.5 convolution_convert_fusion.4
  223.0 1.5 convolution_convert_fusion.5
  224.5 1.5 convolution_convert_fusion.4
  231.6 1.5 convolution_convert_fusion.5
  233.1 1.5 convolution_convert_fusion.4
  241.7 1.5 convolution_convert_fusion.4
  248.8 1.5 convolution_convert_fusion.5
  250.3 1.5 convolution_convert_fusion.4
  257.4 1.5 convolution_convert_fusion.5
  258.9 1.5 convolution_convert_fusion.4
  267.5 1.5 convolution_convert_fusion.4
  276.1 1.5 convolution_convert_fusion.4
  284.7 1.5 convolution_convert_fusion.4
  298.0 2.9 add_convert_fusion
  300.9 34.4 %all_to_all.10 = bf16[8,64,2048]{2,1,0:T(8,128)(2,1)S(1)} all-to-all(bf16[8,64,2048]{2,1,0:T(8,128)(2,1)S(1)} %bitcast.87), channel_id=1, replica_groups=mesh['sp'=32,'tp'=8] {'tp'}, dimensions={0} | all-to-all | bytes 4194304 | tf_op jit(solution)/shard_map/all_to_all | solution.py:67
  (206 shorter events, 88.6 us)
Async XLA Ops:
  6.5 36.6 %copy-start = (bf16[2048,256]{1,0:T(8,128)(2,1)S(1)}, bf16[2048,256]{1,0:T(8,128)(2,1)}, u32[]{:S(2)}) copy-start(bf16[2048,256]{1,0:T(8,128)(2,1)} %param.24) | copy-start | bytes 3145732
  9.2 32.9 %all-to-all-start = ((bf16[8,512,256]{1,2,0:T(8,128)(2,1)}), bf16[8,512,256]{1,2,0:T(8,128)(2,1)S(1)}, u32[]{:S(2)}, u32[]{:S(2)}) async-start(bf16[8,512,256]{1,2,0:T(8,128)(2,1)} %broadcast_in_dim.8), calls=%async_computation | async-start | bytes 4194304 | tf_op jit(solution)/shard_map/all_to_all | solution.py:24
  15.9 26.8 %copy-start.6 = (bf16[2048,32]{0,1:T(8,128)(2,1)S(1)}, bf16[2048,32]{0,1:T(8,128)(2,1)}, u32[]{:S(2)}) copy-start(bf16[2048,32]{0,1:T(8,128)(2,1)} %param.25) | copy-start | bytes 393220
  15.9 136.7 %all-gather.2.cloned.1.call-start = ((), (), s32[]{:S(2)}) async-start(), calls=%async_computation.2 | async-start | bytes 9732096 | tf_op jit(solution)/shard_map/all_gather | solution.py:52
  43.2 0.8 copy-start.7
  43.2 4.6 %copy-start.8 = (bf16[3,128]{1,0:T(4,128)(2,1)S(1)}, bf16[3,128]{1,0:T(4,128)(2,1)}, u32[]{:S(2)}) copy-start(bf16[3,128]{1,0:T(4,128)(2,1)} %param.22) | copy-start | bytes 2308
  47.8 2.1 copy-start.9
  49.9 4.7 %copy-start.3 = (bf16[2048,192]{0,1:T(8,128)(2,1)S(1)}, bf16[2048,192]{0,1:T(8,128)(2,1)}, u32[]{:S(2)}) copy-start(bf16[2048,192]{0,1:T(8,128)(2,1)} %param.23) | copy-start | bytes 2359300
  50.7 4.6 %copy-start.10 = (bf16[2048,128]{1,0:T(8,128)(2,1)S(1)}, bf16[2048,128]{1,0:T(8,128)(2,1)}, u32[]{:S(2)}) copy-start(bf16[2048,128]{1,0:T(8,128)(2,1)} %param.20) | copy-start | bytes 1572868
  50.7 7.1 %collective-permute-start = (bf16[1,128]{1,0:T(2,128)(2,1)S(1)}, bf16[1,128]{1,0:T(2,128)(2,1)S(1)}, u32[]{:S(2)}, u32[]{:S(2)}) collective-permute-start(bf16[1,128]{1,0:T(2,128)(2,1)S(1)} %get-tuple-element.155), channel_id=1, source_target_pairs={{0,8},{8,16},{16,24},{24,32},{32,40},{40,48},{48,56},{56,64},{64,7... | collective-permute-start | bytes 776 | tf_op jit(solution)/shard_map/ppermute | solution.py:41
  53.1 4.7 %collective-permute-start.1 = (bf16[1,128]{1,0:T(2,128)(2,1)S(1)}, bf16[1,128]{1,0:T(2,128)(2,1)S(1)}, u32[]{:S(2)}, u32[]{:S(2)}) collective-permute-start(bf16[1,128]{1,0:T(2,128)(2,1)S(1)} %get-tuple-element.156), channel_id=1, source_target_pairs={{8,0},{16,8},{24,16},{32,24},{40,32},{48,40},{56,48},{64,56},{72,6... | collective-permute-start | bytes 776 | tf_op jit(solution)/shard_map/ppermute | solution.py:43
  55.2 1.0 copy-start.11
  55.3 1.8 copy-start.12
  57.0 1.0 copy-start.4
  152.6 7.7 %slice-start = ((bf16[16384,288]{0,1:T(8,128)(2,1)}), bf16[16384,32]{0,1:T(8,128)(2,1)S(1)}, s32[]{:S(2)}) async-start(bf16[16384,288]{0,1:T(8,128)(2,1)} %all-gather.2.cloned.1.call-done), calls=%async_computation.3 | async-start | bytes 2097152 | tf_op jit(solution)/shard_map/slice | solution.py:54
  152.6 7.7 %copy-start.1 = (bf16[256,128]{1,0:T(8,128)(2,1)S(1)}, bf16[256,128]{1,0:T(8,128)(2,1)}, u32[]{:S(2)}) copy-start(bf16[256,128]{1,0:T(8,128)(2,1)} %param.27) | copy-start | bytes 196612
  152.6 7.7 %copy-start.2 = (bf16[256,128]{1,0:T(8,128)(2,1)S(1)}, bf16[256,128]{1,0:T(8,128)(2,1)}, u32[]{:S(2)}) copy-start(bf16[256,128]{1,0:T(8,128)(2,1)} %param.28) | copy-start | bytes 196612
  160.3 137.7 %copy-start.5 = (bf16[128,2048]{1,0:T(8,128)(2,1)S(1)}, bf16[128,2048]{1,0:T(8,128)(2,1)}, u32[]{:S(2)}) copy-start(bf16[128,2048]{1,0:T(8,128)(2,1)} %param.31) | copy-start | bytes 1572868
Sparse Core Ops, SparseCore 0:
  47.9 104.6 all-gather.1
where the time goes:
time: 346 us; the launch traced here: 343 us
  waiting for transfers between devices  118 us (34%)
  matrix products  98.8 us (29%)
  blocking collectives  34.4 us (10%)
  loops' own time  31.7 us (9%)
  local copies, waits for them, and re-layouts  20.7 us (6%)
  other arithmetic  15.3 us (4%)
  between operations  13.7 us (4%)
  starting transfers between devices  10.6 us (3%)
    all_gather x1, waiting for transfers between devices, sent_together(): lax.all_gather(both, axis, axis=dim, tiled=True)  91.8 us
    all_to_all x1, blocking collectives, sum_at_owner(): lax.all_to_all(parts, axis, split_axis=0, concat_axis=0, tiled=True)  34.4 us
    another operation x1, loops' own time, on_device(): gathered_state = lax.scan(one_span, initial, span_starts)[0]  31.7 us
    all_to_all x1, waiting for transfers between devices, sent_to_all(): lax.all_to_all(jnp.broadcast_to(value[None], (length, *value.shape)), axi...  26.2 us
    dot_general x16, matrix products, one_span(): jnp.dot(latent_span, key_up, preferred_element_type=jnp.float32)  23.7 us
    dot_general x16, matrix products, one_span(): jnp.dot(latent_span, value_up, preferred_element_type=jnp.float32)  23.7 us
    dot_general x16, matrix products, one_span(): jnp.einsum('qhd,kd->qhk', query_rope, rope_span, preferred_element_type=j...  14.3 us
    dot_general x16, matrix products, one_span(): jnp.einsum('qhk,khd->qhd', weights.astype(jnp.bfloat16), key_values, pref...  12.9 us
  transfers between devices with their start and end apart: 4, of which 2 were waited for; matrix products, arithmetic and copies ran while one was open for 2% of the time, Pallas kernels for 0%

commit v1 on v0

v1 whole, which is shorter than its diff:
```python
import math

import jax
import jax.numpy as jnp
from jax import lax
from jax.experimental import pallas as pl
from jax.experimental.pallas import tpu as pltpu
from jax.sharding import PartitionSpec as P

NOPE, ROPE, VDIM, GRID_W = 64, 32, 64, 64
EPS = 1e-06
THETA = 10000.0
D = 2048
T = 512
FB = 256
NX, NY, NZ = 4, 4, 8
KEYS = NZ * T
PIECE = T + 64
HALF = PIECE // 2
SUB = HALF // 2
VROWS = VDIM + 16
CHUNK = 512
N_REMOTE = 80
N_LOCAL = 16
MESH = pl.DeviceIdType.MESH
F32, BF16 = jnp.float32, jnp.bfloat16


def iota(shape, dim):
    return lax.broadcasted_iota(jnp.int32, shape, dim)


def mm(a, b):
    return jnp.dot(a, b, preferred_element_type=F32)


def silu(v):
    return v * (1.0 / (1.0 + jnp.exp(-v)))


def selection(rows, cols, test):
    return jnp.where(test(iota((rows, cols), 0), iota((rows, cols), 1)), 1.0, 0.0).astype(BF16)


def layer_kernel(
    tokens, conv_input, conv_inner, conv_outer, conv_gate, conv_taps, query_proj, latent_proj,
    rope_proj, latent_gain, key_up, value_up, attn_gate, conv_down, attn_down,
    out,
    xall, w5, wq_raw, wq, wl, wr_raw, wr, ku_raw, ku2, vu_raw, wd, taps, gain,
    a5, al, aq, ar, ss, cos_t, sin_t,
    msg, qs, kall, vt, sbuf, acc,
    om, ostat, ro, rstat, relay, relay_stat,
    cprod, halo, conv_out, lhs, p_send, p_recv, own, pair2, pair1, pair3, turn_a, turn_b, from_l, from_r,
    send_sems, recv_sems, local_sems,
):
    sp, tp = lax.axis_index("sp"), lax.axis_index("tp")
    z, y = sp // NY, sp % NY
    x, core = tp // 2, tp % 2
    other = 1 - core
    dev = lambda s, t: {"sp": s, "tp": t}
    partner = dev(sp, x * 2 + other)
    xr, xl = dev(sp, (x + 1) % NX * 2 + core), dev(sp, (x + NX - 1) % NX * 2 + core)
    yr, yl = dev(z * NY + (y + 1) % NY, tp), dev(z * NY + (y + NY - 1) % NY, tp)
    zr, zl = dev((z + 1) % NZ * NY + y, tp), dev((z + NZ - 1) % NZ * NY + y, tp)
    span_next, span_prev = dev((sp + 1) % (NZ * NY), tp), dev((sp + NZ * NY - 1) % (NZ * NY), tp)

    started = []

    def remote(src, dst, to):
        k = len(started)
        copy = pltpu.make_async_remote_copy(
            src_ref=src, dst_ref=dst, send_sem=send_sems.at[k], recv_sem=recv_sems.at[k],
            device_id=to, device_id_type=MESH,
        )
        copy.start()
        started.append(copy)
        return copy

    locals_ = []

    def load(src, dst):
        copy = pltpu.make_async_copy(src, dst, local_sems.at[len(locals_)])
        copy.start()
        locals_.append(copy)
        return copy

    own_block = load(tokens, xall.at[0])
    loads_rope = [load(rope_proj, wr_raw), load(query_proj, wq_raw), load(key_up, ku_raw), load(value_up, vu_raw)]
    loads_proj = [
        load(w, w5.at[:, pl.ds(128 * k, 128)])
        for k, w in enumerate((conv_input, conv_inner, conv_outer, conv_gate, attn_gate))
    ]
    loads_proj.append(load(latent_proj, wl))
    loads_late = [load(conv_taps, taps), load(latent_gain, gain)]
    loads_late += [load(conv_down, wd.at[pl.ds(0, 128), :]), load(attn_down, wd.at[pl.ds(128, 128), :])]

    barrier = pltpu.get_barrier_semaphore()
    peers = (partner, xr, xl, yr, yl, zr, zl, span_next, span_prev)
    for to in peers:
        pl.semaphore_signal(barrier, inc=1, device_id=to, device_id_type=MESH)
    pl.semaphore_wait(barrier, len(peers))

    own_block.wait()
    h0, h1 = pl.ds(0, T // 2), pl.ds(T // 2, T // 2)
    r0 = remote(xall.at[0, h0], xall.at[1, h0], xr)
    l0 = remote(xall.at[0, h1], xall.at[2, h1], xl)
    r1 = remote(xall.at[0, h1], xall.at[1, h1], xr)
    l1 = remote(xall.at[0, h0], xall.at[2, h0], xl)
    d0 = remote(xall.at[0], xall.at[4], partner)

    for c in loads_rope:
        c.wait()
    e_q = selection(192, 256, lambda r, c: (c % 128 < 96) & (r == c // 128 * 96 + c % 128))

    def widen(i, _):
        rows = pl.ds(pl.multiple_of(i * 256, 256), 256)
        wq[rows, :] = mm(wq_raw[rows, :], e_q).astype(BF16)
        wr[rows, :] = mm(wr_raw[rows, :], selection(32, 128, lambda r, c: r == c)).astype(BF16)
        return 0

    lax.fori_loop(0, D // 256, widen, 0)
    ku2[...] = mm(
        ku_raw[...], selection(128, 256, lambda r, c: (c % 128 < 64) & (r == c // 128 * 64 + c % 128))
    ).astype(BF16)
    token = iota((T, 128), 0) + sp * T
    lane = iota((T, 128), 1)
    freq = jnp.zeros((T, 128), F32)
    for j in range(8):
        freq = jnp.where(lane % 8 == j, float(THETA ** (-2.0 * j / 16)), freq)
    grid_at = jnp.where(lane % 32 < 16, token // GRID_W, token % GRID_W).astype(F32)
    angle = grid_at * freq
    cos_t[...] = jnp.cos(angle)
    sin_t[...] = jnp.sin(angle) * jnp.where(lane % 16 < 8, -1.0, 1.0)
    for i in range(NY):
        for h in range(2):
            qs[i, h, pl.ds(96, 32), :] = jnp.zeros((32, T), BF16)
    for h in range(2):
        vt[h, pl.ds(VDIM, 16), :] = jnp.where(iota((16, KEYS), 0) == 0, 1.0, 0.0).astype(BF16)
    for c in loads_proj:
        c.wait()

    def project(slot, chip, c, first=False):
        block = pl.multiple_of((chip * 2 + c) * FB, FB)

        def rows_of(i, _):
            rows = pl.ds(pl.multiple_of(i * 256, 256), 256)
            v = xall[slot, rows, :]
            wide = v.astype(F32)
            squares = wide[:, :128] * wide[:, :128] + wide[:, 128:] * wide[:, 128:]
            for total, w in ((a5, w5), (al, wl), (aq, wq), (ar, wr)):
                term = mm(v, w[pl.ds(block, FB), :])
                total[rows, :] = term if first else total[rows, :] + term
            ss[rows, :] = squares if first else ss[rows, :] + squares
            return 0

        lax.fori_loop(0, T // 256, rows_of, 0)

    left, right, across = (x + NX - 1) % NX, (x + 1) % NX, (x + 2) % NX
    r0.wait_recv()
    r2 = remote(xall.at[1, h0], xall.at[3, h0], xr)
    l0.wait_recv()
    l2 = remote(xall.at[2, h1], xall.at[3, h1], xl)
    project(0, x, core, first=True)
    d0.wait_recv()
    project(4, x, other)
    r1.wait_recv()
    d1 = remote(xall.at[1], xall.at[5], partner)
    l1.wait_recv()
    d2 = remote(xall.at[2], xall.at[6], partner)
    project(1, left, core)
    project(2, right, core)
    d1.wait_recv()
    project(5, left, other)
    d2.wait_recv()
    project(6, right, other)
    r2.wait_recv()
    d3a = remote(xall.at[3, h0], xall.at[7, h0], partner)
    l2.wait_recv()
    d3b = remote(xall.at[3, h1], xall.at[7, h1], partner)
    project(3, across, core)
    d3a.wait_recv()
    d3b.wait_recv()
    project(7, across, other)
    for c in loads_late:
        c.wait()

    scale = lax.rsqrt(jnp.sum(ss[...], axis=1, keepdims=True) / D + EPS)
    zl_ = al[...] * scale
    latent = zl_ * lax.rsqrt(jnp.mean(zl_ * zl_, axis=1, keepdims=True) + EPS) * gain[...].reshape(1, 256)
    latent = latent.astype(BF16)
    msg[0, 0] = latent[:HALF]
    msg[0, 1, pl.ds(0, T - HALF), :] = latent[HALF:]

    def turned(v):
        swapped = jnp.where(lane % 16 < 8, pltpu.roll(v, 120, 1), pltpu.roll(v, 8, 1))
        return v * cos_t[...] + swapped * sin_t[...]

    key_rope = turned(ar[...] * scale).astype(BF16)
    packed = jnp.zeros((128, 128), F32)
    for g in range(4):
        place = selection(128, 128, lambda r, c, g=g: (r < 32) & (c == r + 32 * g))
        packed = packed + mm(key_rope[128 * g : 128 * (g + 1)], place)
    packed = packed.astype(BF16)
    msg[0, 1, pl.ds(T - HALF, 64), pl.ds(0, 128)] = packed[:64]
    msg[0, 1, pl.ds(T - HALF, 64), pl.ds(128, 128)] = packed[64:]

    s0, s1 = pl.ds(0, SUB), pl.ds(SUB, SUB)

    def key_send(step, sub, to_right):
        d_from, d_to = (step, step + 1) if to_right else ((NZ - step) % NZ, NZ - 1 - step)
        return remote(msg.at[d_from, core, sub], msg.at[d_to, core, sub], zr if to_right else zl)

    zr_a, zl_b = key_send(0, s0, True), key_send(0, s1, False)
    zr_b, zl_a = key_send(0, s1, True), key_send(0, s0, False)

    q_scale = scale * ((NOPE + ROPE) ** (-0.5) * math.log2(math.e))
    for h in range(2):
        v = aq[:, 128 * h : 128 * (h + 1)] * q_scale
        v = jnp.where((lane >= 64) & (lane < 96), turned(v), v)
        qs[0, h, pl.ds(0, 96), :] = jnp.transpose(v)[:96].astype(BF16)
    q96 = pl.ds(0, 96)
    qr0 = remote(qs.at[0, 0, q96], qs.at[1, 0, q96], yr)
    ql0 = remote(qs.at[0, 1, q96], qs.at[2, 1, q96], yl)
    qr1 = remote(qs.at[0, 1, q96], qs.at[1, 1, q96], yr)
    ql1 = remote(qs.at[0, 0, q96], qs.at[2, 0, q96], yl)

    rounded = lambda k: (a5[:, 128 * k : 128 * (k + 1)] * scale).astype(BF16).astype(F32)
    cprod[...] = (rounded(1) * rounded(0)).astype(BF16)
    to_next = remote(cprod.at[pl.ds(T - 16, 16)], halo.at[0], span_next)
    to_prev = remote(cprod.at[pl.ds(0, 16)], halo.at[1], span_prev)

    vu_t = jnp.transpose(vu_raw[...].astype(F32)).astype(BF16)
    e_k = [
        selection(128, 256, lambda r, c, g=g: (c % 128 >= 64) & (c % 128 < 96) & (r == 32 * g + c % 128 - 64))
        for g in range(4)
    ]

    def build(d):
        piece = jnp.concatenate([msg[d, 0], msg[d, 1]], axis=0)
        lat, pk = piece[:T], piece[T:]
        pk = jnp.concatenate([pk[:, :128], pk[:, 128:]], axis=0)
        for g in range(4):
            k = mm(lat[128 * g : 128 * (g + 1)], ku2[...]) + mm(pk, e_k[g])
            kall[pl.ds(d * T + 128 * g, 128), :] = k.astype(BF16)
        v = lax.dot_general(vu_t, lat, (((1,), (1,)), ((), ())), preferred_element_type=F32).astype(BF16)
        for h in range(2):
            vt[h, pl.ds(0, VDIM), pl.ds(d * T, T)] = v[VDIM * h : VDIM * (h + 1)]

    build(0)

    swaps = {}
    for step in range(1, 4):
        zr_a.wait_recv()
        nr_a = key_send(step, s0, True)
        zl_b.wait_recv()
        nl_b = key_send(step, s1, False)
        zr_b.wait_recv()
        zl_a.wait_recv()
        if step < 3:
            nr_b, nl_a = key_send(step, s1, True), key_send(step, s0, False)
        for d in (step, NZ - step):
            swaps[d] = remote(msg.at[d, core], msg.at[d, core], partner)
        if step == 1:
            qr0.wait_recv()
            qr2 = remote(qs.at[1, 0, q96], qs.at[3, 0, q96], yr)
            ql0.wait_recv()
            ql2 = remote(qs.at[2, 1, q96], qs.at[3, 1, q96], yl)
        else:
            for d in (step - 1, NZ - step + 1):
                swaps[d].wait_recv()
                build(d)
        zr_a, zl_b = nr_a, nl_b
        if step < 3:
            zr_b, zl_a = nr_b, nl_a
    for d in (3, 5):
        swaps[d].wait_recv()
        build(d)
    zr_a.wait_recv()
    zl_b.wait_recv()
    swaps[4] = remote(msg.at[4, core], msg.at[4, core], partner)

    to_next.wait_recv()
    to_prev.wait_recv()
    cp = cprod[...].astype(F32)
    row = iota((T, 128), 0)
    before = jnp.where(sp > 0, halo[0].astype(F32)[15:16], 0.0)
    after = jnp.where(sp < NY * NZ - 1, halo[1].astype(F32)[0:1], 0.0)
    tap = taps[...].astype(F32)
    mixed = (
        jnp.where(row == 0, before, pltpu.roll(cp, 1, 0)) * tap[0:1]
        + cp * tap[1:2]
        + jnp.where(row == T - 1, after, pltpu.roll(cp, T - 1, 0)) * tap[2:3]
    )
    conv_out[...] = (silu(rounded(3)) * rounded(2) * mixed).astype(BF16)
    gate = silu(rounded(4))

    swaps[4].wait_recv()
    build(4)
    for c in (qr1, ql1, qr2, ql2):
        c.wait_recv()

    def stage(new, old, m_old):
        def body(j, mx):
            keys = pl.ds(pl.multiple_of(j * CHUNK, CHUNK), CHUNK)
            if new is not None:
                i, h = new
                s = mm(kall[keys, 128 * h : 128 * (h + 1)], qs[i, h])
                sbuf[h, keys, :] = s
                mx = jnp.maximum(mx, jnp.max(s.reshape(CHUNK // 8, 8, T), axis=0))
            if old is not None:
                g = old[1]
                p = jnp.exp2(sbuf[g, keys, :] - m_old).astype(BF16)
                acc[...] += mm(vt[g, :, keys], p)
            return mx

        if old is not None:
            acc[...] = jnp.zeros_like(acc)
        mx = lax.fori_loop(0, KEYS // CHUNK, body, jnp.full((8, T), -jnp.inf, F32))
        return jnp.max(mx, axis=0, keepdims=True)

    def finish(unit, m):
        i, h = unit
        total = acc[pl.ds(VDIM, 1), :]
        om[i, h] = (acc[pl.ds(0, VDIM), :] * (1.0 / total)).astype(BF16)
        ostat[i, h] = jnp.where(iota((8, T), 0) == 0, m, total)

    units = [(i, h) for i in (3, 2, 1, 0) for h in range(2)]
    back = {}
    m_now = stage(units[0], None, None)
    for n, unit in enumerate(units):
        following = units[n + 1] if n + 1 < len(units) else None
        m_next = stage(following, unit, m_now)
        finish(unit, m_now)
        m_now = m_next
        i, h = unit
        if i == 3:
            to = xr_y = yr if h == 0 else yl
            back[unit] = (remote(om.at[i, h], relay.at[h], to), remote(ostat.at[i, h], relay_stat.at[h], to))
        elif i in (1, 2):
            to, slot = (yl, 2) if i == 1 else (yr, 1)
            back[unit] = (remote(om.at[i, h], ro.at[slot, h], to), remote(ostat.at[i, h], rstat.at[slot, h], to))
        if i == 2:
            for c in back[(3, h)]:
                c.wait_recv()
            to = yr if h == 0 else yl
            back[(0, h)] = (remote(relay.at[h], ro.at[3, h], to), remote(relay_stat.at[h], rstat.at[3, h], to))
    for cs in [v for k, v in back.items() if k[0] != 3]:
        for c in cs:
            c.wait_recv()
    parts = []
    for h in range(2):
        os = [om[0, h]] + [ro[k, h] for k in (1, 2, 3)]
        st = [ostat[0, h]] + [rstat[k, h] for k in (1, 2, 3)]
        top = st[0][0:1]
        for s in st[1:]:
            top = jnp.maximum(top, s[0:1])
        weights = [s[1:2] * jnp.exp2(s[0:1] - top) for s in st]
        total = weights[0] + weights[1] + weights[2] + weights[3]
        summed = os[0].astype(F32) * weights[0]
        for o, w in zip(os[1:], weights[1:]):
            summed = summed + o.astype(F32) * w
        parts.append(summed / total)
    attended = jnp.transpose(jnp.concatenate(parts, axis=0))
    attn_out = (gate * attended).astype(BF16)
    for chip in range(NX):
        for c in range(2):
            rows = slice(128 * chip + 64 * c, 128 * chip + 64 * (c + 1))
            lhs[chip, c, :, pl.ds(0, 128)] = conv_out[rows, :]
            lhs[chip, c, :, pl.ds(128, 128)] = attn_out[rows]

    order = (2, 1, 3, 0)
    to_partner = {}
    for r in order:
        p_send[r] = mm(lhs[(x + r) % NX, other], wd[...]).astype(BF16)
        to_partner[r] = remote(p_send.at[r], p_recv.at[r], partner)
    for r in order:
        own[r] = mm(lhs[(x + r) % NX, core], wd[...])
    lo, hi = slice(0, 1024), slice(1024, 2048)
    to_partner[2].wait_recv()
    for k, cols in enumerate((lo, hi)):
        pair2[k] = (own[2, :, cols] + p_recv[2, :, cols].astype(F32)).astype(BF16)
    ta = remote(pair2.at[0], turn_a, xr)
    tb = remote(pair2.at[1], turn_b, xl)
    to_partner[1].wait_recv()
    pair1[1] = (own[1, :, hi] + p_recv[1, :, hi].astype(F32)).astype(BF16)
    far_r = remote(pair1.at[1], from_l.at[1], xr)
    to_partner[3].wait_recv()
    pair3[0] = (own[3, :, lo] + p_recv[3, :, lo].astype(F32)).astype(BF16)
    far_l = remote(pair3.at[0], from_r.at[0], xl)
    ta.wait_recv()
    pair1[0] = (own[1, :, lo] + p_recv[1, :, lo].astype(F32) + turn_a[...].astype(F32)).astype(BF16)
    near_r = remote(pair1.at[0], from_l.at[0], xr)
    tb.wait_recv()
    pair3[1] = (own[3, :, hi] + p_recv[3, :, hi].astype(F32) + turn_b[...].astype(F32)).astype(BF16)
    near_l = remote(pair3.at[1], from_r.at[1], xl)
    to_partner[0].wait_recv()
    far_r.wait_recv()
    far_l.wait_recv()
    near_r.wait_recv()
    near_l.wait_recv()
    for k, cols in enumerate((lo, hi)):
        out[:, cols] = (
            own[0, :, cols] + p_recv[0, :, cols].astype(F32) + from_l[k].astype(F32) + from_r[k].astype(F32)
        ).astype(BF16)
    for c in started:
        c.wait_send()


def scratch():
    v = lambda shape, kind=BF16: pltpu.VMEM(shape, kind)
    return [
        v((8, T, FB)), v((D, 640)), v((D, 192)), v((D, 256)), v((D, 256)), v((D, 32)), v((D, 128)),
        v((256, 128)), v((256, 256)), v((256, 128)), v((256, D)), v((3, 128)), v((256,), F32),
        v((T, 640), F32), v((T, 256), F32), v((T, 256), F32), v((T, 128), F32), v((T, 128), F32),
        v((T, 128), F32), v((T, 128), F32),
        v((NZ, 2, HALF, 256)), v((NY, 2, 128, T)), v((KEYS, 256)), v((2, VROWS, KEYS)),
        v((2, KEYS, T), F32), v((VROWS, T), F32),
        v((NY, 2, VDIM, T)), v((NY, 2, 8, T), F32), v((NY, 2, VDIM, T)), v((NY, 2, 8, T), F32),
        v((2, VDIM, T)), v((2, 8, T), F32),
        v((T, 128)), v((2, 16, 128)), v((T, 128)), v((NX, 2, 64, 256)),
        v((NX, 64, D)), v((NX, 64, D)), v((NX, 64, D), F32),
        v((2, 64, 1024)), v((2, 64, 1024)), v((2, 64, 1024)), v((64, 1024)), v((64, 1024)),
        v((2, 64, 1024)), v((2, 64, 1024)),
        pltpu.SemaphoreType.DMA((N_REMOTE,)), pltpu.SemaphoreType.DMA((N_REMOTE,)),
        pltpu.SemaphoreType.DMA((N_LOCAL,)),
    ]


def on_device(*args):
    return pl.pallas_call(
        layer_kernel,
        out_shape=jax.ShapeDtypeStruct((64, D), BF16),
        in_specs=[pl.BlockSpec(memory_space=pl.ANY)] * len(args),
        out_specs=pl.BlockSpec(memory_space=pltpu.VMEM),
        scratch_shapes=scratch(),
        compiler_params=pltpu.CompilerParams(
            collective_id=0, has_side_effects=True, vmem_limit_bytes=62 * 1024 * 1024
        ),
        name="layer",
    )(*args)


def solution(mesh):
    cols, rows, whole = P(None, "tp"), P("tp", None), P()
    placed = (P("sp", "tp"), cols, cols, cols, cols, cols, cols, whole, whole, whole, cols, cols, cols, rows, rows)
    return jax.shard_map(
        on_device, mesh=mesh, in_specs=placed, out_specs=P(("sp", "tp"), None), check_vma=False
    )
```

time: 346 us -> 87.1 us (0.25)
  waiting for transfers between devices: 118 us -> 0 us
  matrix products: 98.8 us -> 0 us
  Pallas kernels: 0 us -> 81.2 us
  blocking collectives: 34.4 us -> 0 us
  loops' own time: 31.7 us -> 0 us
  other arithmetic: 15.3 us -> 0 us
  local copies, waits for them, and re-layouts: 20.7 us -> 5.83 us
  between operations: 13.7 us -> 0.01 us
  starting transfers between devices: 10.6 us -> 0 us
    dot_general x90 -> x0, matrix products: 98.8 us -> none  [the longest x16 23.7 us: one_span(): jnp.dot(latent_span, key_up, preferred_element_type=jnp.float32)]
    all_gather x1 -> x0, waiting for transfers between devices: 91.8 us -> none  [sent_together(): lax.all_gather(both, axis, axis=dim, tiled=True)]
    pallas_call x0 -> x1, Pallas kernels: none -> 81.2 us  [on_device(): pl.pallas_call(layer_kernel, out_shape=jax.ShapeDtypeStruct((64, D), BF16...]
    all_to_all x1 -> x0, blocking collectives: 34.4 us -> none  [sum_at_owner(): lax.all_to_all(parts, axis, split_axis=0, concat_axis=0, tiled=True)]
    another operation x1 -> x0, loops' own time: 31.7 us -> none  [on_device(): gathered_state = lax.scan(one_span, initial, span_starts)[0]]
    all_to_all x1 -> x0, waiting for transfers between devices: 26.2 us -> none  [sent_to_all(): lax.all_to_all(jnp.broadcast_to(value[None], (length, *value.shape)), axi...]
    reduce_sum x18 -> x0, other arithmetic: 10.8 us -> none  [the longest x16 9.15 us: one_span(): weight_total = weight_total * shrink + jnp.sum(weights, axis=2)]
    dynamic_slice x16 -> x0, local copies, waits for them, and re-layouts: 9.73 us -> none  [on_device(): gathered_state = lax.scan(one_span, initial, span_starts)[0]]
  transfers between devices with their start and end apart: 4 -> 0, of which waited for: 2 -> 0; matrix products, arithmetic and copies ran while one was open for 2% -> 0% of each run, Pallas kernels for 0% -> 0%
where the time goes in v1:
time: 87.1 us; the launch traced here: 87 us
  Pallas kernels  81.2 us (93%)
  local copies, waits for them, and re-layouts  5.83 us (7%)
    pallas_call x1, Pallas kernels, on_device(): pl.pallas_call(layer_kernel, out_shape=jax.ShapeDtypeStruct((64, D), BF16...  81.2 us
    unnamed x3, local copies, waits for them, and re-layouts  5.83 us

profile of v1, /device:TPU:1, one launch (start us, length us, event | category | flops | bytes accessed | tf_op | source)
XLA Modules:
  0.0 87.0 jit_solution(5101072249401870539)
XLA Ops:
  0.0 1.9 %copy.17.rope_proj = bf16[2048,32]{1,0:T(8,128)(2,1)} copy(bf16[2048,32]{0,1:T(8,128)(2,1)} %param.23) | data formatting | bytes 262144 | tf_op args[8]
  1.9 2.2 %copy.16.query_proj = bf16[2048,192]{1,0:T(8,128)(2,1)} copy(bf16[2048,192]{0,1:T(8,128)(2,1)} %param.21) | data formatting | bytes 1572864 | tf_op args[6]
  4.2 81.2 %layer.1 = bf16[64,2048]{1,0:T(8,128)(2,1)} custom-call(bf16[512,256]{1,0:T(8,128)(2,1)} %tokens.1, bf16[2048,128]{1,0:T(8,128)(2,1)} %conv_input.1, bf16[2048,128]{1,0:T(8,128)(2,1)} %conv_inner.1, bf16[2048,128]{1,0:T(8,128)(2,1)} %conv_outer.1, bf16[2048,128]{1,0:T(8,128)(2,1)} %conv_gate.1, bf16[3,128]{1,0:T(4,128)(2,1)} %conv_taps.1, ...), custom_call_target="tpu_custom_call" | custom-call | tf_op jit(solution)/shard_map/layer/pallas_call | solution.py:430
  85.3 1.7 %copy.19 = bf16[64,2048]{1,0:T(8,128)(2,1)} copy(bf16[64,2048]{1,0:T(8,128)(2,1)} %layer.1) | data formatting | bytes 524288

commit v2 on v1

v2 whole, which is shorter than its diff:
```python
import math

import jax
import jax.numpy as jnp
from jax import lax
from jax.experimental import pallas as pl
from jax.experimental.pallas import tpu as pltpu
from jax.sharding import PartitionSpec as P

NOPE, ROPE, VDIM, GRID_W = 64, 32, 64, 64
EPS = 1e-06
THETA = 10000.0
D = 2048
T = 512
FB = 256
NX, NY, NZ = 4, 4, 8
KEYS = NZ * T
PIECE = T + 64
HALF = PIECE // 2
SUB = HALF // 2
VROWS = VDIM + 16
CHUNK = 512
ARRIVAL = (0, 1, 7, 2, 6, 3, 5, 4)
N_REMOTE = 96
N_LOCAL = 16
MESH = pl.DeviceIdType.MESH
F32, BF16 = jnp.float32, jnp.bfloat16


def iota(shape, dim):
    return lax.broadcasted_iota(jnp.int32, shape, dim)


def mm(a, b):
    return jnp.dot(a, b, preferred_element_type=F32)


def silu(v):
    return v * (1.0 / (1.0 + jnp.exp(-v)))


def selection(rows, cols, test):
    return jnp.where(test(iota((rows, cols), 0), iota((rows, cols), 1)), 1.0, 0.0).astype(BF16)


def layer_kernel(
    tokens, conv_input, conv_inner, conv_outer, conv_gate, conv_taps, query_proj, latent_proj,
    rope_proj, latent_gain, key_up, value_up, attn_gate, conv_down, attn_down,
    out,
    xall, w5, wqr, wl, ku_raw, ku2, vu_raw, wd, taps, gain,
    a5, al, aqr, ss,
    msg, qs, kall, vt, sbuf, acc, tops,
    om, ostat, ro, rstat, relay, relay_stat, both, both_stat,
    wall, aout, aall, cprod, halo, conv_out, gate_out, p_send, p_recv, own, pair2, pair1, pair3, turn_a, turn_b, from_l, from_r,
    send_sems, recv_sems, local_sems,
):
    sp, tp = lax.axis_index("sp"), lax.axis_index("tp")
    z, y = sp // NY, sp % NY
    x, core = tp // 2, tp % 2
    other = 1 - core
    dev = lambda s, t: {"sp": s, "tp": t}
    partner = dev(sp, x * 2 + other)
    xr, xl = dev(sp, (x + 1) % NX * 2 + core), dev(sp, (x + NX - 1) % NX * 2 + core)
    yr, yl = dev(z * NY + (y + 1) % NY, tp), dev(z * NY + (y + NY - 1) % NY, tp)
    zr, zl = dev((z + 1) % NZ * NY + y, tp), dev((z + NZ - 1) % NZ * NY + y, tp)
    span_next, span_prev = dev((sp + 1) % (NZ * NY), tp), dev((sp + NZ * NY - 1) % (NZ * NY), tp)

    started = []

    def remote(src, dst, to):
        k = len(started)
        copy = pltpu.make_async_remote_copy(
            src_ref=src, dst_ref=dst, send_sem=send_sems.at[k], recv_sem=recv_sems.at[k],
            device_id=to, device_id_type=MESH,
        )
        copy.start()
        started.append(copy)
        return copy

    locals_ = []

    def load(src, dst):
        copy = pltpu.make_async_copy(src, dst, local_sems.at[len(locals_)])
        copy.start()
        locals_.append(copy)
        return copy

    own_block = load(tokens, xall.at[0])
    loads_proj = [load(query_proj, wqr.at[pl.ds(0, 192), :]), load(rope_proj, wqr.at[pl.ds(192, ROPE), :])]
    loads_proj += [
        load(w, w5.at[:, pl.ds(128 * k, 128)])
        for k, w in enumerate((conv_input, conv_inner, conv_outer, conv_gate, attn_gate))
    ]
    loads_proj.append(load(latent_proj, wl))
    loads_late = [load(conv_taps, taps), load(latent_gain, gain), load(key_up, ku_raw), load(value_up, vu_raw)]
    loads_late += [load(conv_down, wd), load(attn_down, wall.at[0, 0])]

    barrier = pltpu.get_barrier_semaphore()
    tp_peer = lambda r, c: dev(sp, (x + r) % NX * 2 + c)
    peers = [tp_peer(r, c) for r in (1, 2, 3) for c in (core, other)]
    peers += [partner, yr, yl, zr, zl, span_next, span_prev]
    for to in peers:
        pl.semaphore_signal(barrier, inc=1, device_id=to, device_id_type=MESH)
    pl.semaphore_wait(barrier, len(peers))

    own_block.wait()
    h0, h1 = pl.ds(0, T // 2), pl.ds(T // 2, T // 2)
    r0 = remote(xall.at[0, h0], xall.at[1, h0], xr)
    l0 = remote(xall.at[0, h1], xall.at[2, h1], xl)
    r1 = remote(xall.at[0, h1], xall.at[1, h1], xr)
    l1 = remote(xall.at[0, h0], xall.at[2, h0], xl)
    d0 = remote(xall.at[0], xall.at[4], partner)

    token = iota((8, T), 1) + sp * T
    entry = iota((8, T), 0)
    freq = jnp.zeros((8, T), F32)
    for j in range(8):
        freq = jnp.where(entry == j, float(THETA ** (-2.0 * j / 16)), freq)
    row_angle = (token // GRID_W).astype(F32) * freq
    col_angle = (token % GRID_W).astype(F32) * freq
    tables = (jnp.cos(row_angle), jnp.sin(row_angle), jnp.cos(col_angle), jnp.sin(col_angle))
    for i in range(NY):
        for h in range(2):
            qs[i, h, pl.ds(96, 32), :] = jnp.zeros((32, T), BF16)
    for h in range(2):
        vt[h, pl.ds(VDIM, 16), :] = jnp.where(iota((16, KEYS), 0) == 0, 1.0, 0.0).astype(BF16)
    for c in loads_proj:
        c.wait()

    def project(slot, chip, c, first=False):
        block = pl.multiple_of((chip * 2 + c) * FB, FB)

        def rows_of(i, _):
            rows = pl.ds(pl.multiple_of(i * 256, 256), 256)
            v = xall[slot, rows, :]
            wide = v.astype(F32)
            squares = wide[:, :128] * wide[:, :128] + wide[:, 128:] * wide[:, 128:]
            for total, w in ((a5, w5), (al, wl)):
                term = mm(v, w[pl.ds(block, FB), :])
                total[rows, :] = term if first else total[rows, :] + term
            term = lax.dot_general(
                wqr[:, pl.ds(block, FB)], v, (((1,), (1,)), ((), ())), preferred_element_type=F32
            )
            aqr[:, rows] = term if first else aqr[:, rows] + term
            ss[rows, :] = squares if first else ss[rows, :] + squares
            return 0

        lax.fori_loop(0, T // 256, rows_of, 0)

    left, right, across = (x + NX - 1) % NX, (x + 1) % NX, (x + 2) % NX
    r0.wait_recv()
    r2 = remote(xall.at[1, h0], xall.at[3, h0], xr)
    l0.wait_recv()
    l2 = remote(xall.at[2, h1], xall.at[3, h1], xl)
    project(0, x, core, first=True)
    d0.wait_recv()
    project(4, x, other)
    r1.wait_recv()
    d1 = remote(xall.at[1], xall.at[5], partner)
    l1.wait_recv()
    d2 = remote(xall.at[2], xall.at[6], partner)
    project(1, left, core)
    project(2, right, core)
    d1.wait_recv()
    project(5, left, other)
    r2.wait_recv()
    d3a = remote(xall.at[3, h0], xall.at[7, h0], partner)
    l2.wait_recv()
    d3b = remote(xall.at[3, h1], xall.at[7, h1], partner)
    d2.wait_recv()
    project(6, right, other)
    project(3, across, core)
    d3a.wait_recv()
    d3b.wait_recv()
    project(7, across, other)
    for c in loads_late:
        c.wait()

    scale = lax.rsqrt(jnp.sum(ss[...], axis=1, keepdims=True) / D + EPS)
    zl_ = al[...] * scale
    latent = zl_ * lax.rsqrt(jnp.mean(zl_ * zl_, axis=1, keepdims=True) + EPS) * gain[...].reshape(1, 256)
    latent = latent.astype(BF16)
    msg[0, 0] = latent[:HALF]
    msg[0, 1, pl.ds(0, T - HALF), :] = latent[HALF:]

    def turned(v):
        a, b, c, d = v[0:8], v[8:16], v[16:24], v[24:32]
        cos_r, sin_r, cos_c, sin_c = tables
        return jnp.concatenate(
            [a * cos_r - b * sin_r, b * cos_r + a * sin_r, c * cos_c - d * sin_c, d * cos_c + c * sin_c], axis=0
        )

    scale_row = lax.rsqrt(jnp.sum(jnp.transpose(ss[...]), axis=0, keepdims=True) / D + EPS)
    key_rope = turned(aqr[pl.ds(192, ROPE), :] * scale_row).astype(BF16)
    msg[0, 1, pl.ds(T - HALF, ROPE), :] = key_rope[:, :256]
    msg[0, 1, pl.ds(T - HALF + ROPE, ROPE), :] = key_rope[:, 256:]

    s0, s1 = pl.ds(0, SUB), pl.ds(SUB, SUB)

    def key_send(step, sub, to_right):
        d_from, d_to = (step, step + 1) if to_right else ((NZ - step) % NZ, NZ - 1 - step)
        return remote(msg.at[d_from, core, sub], msg.at[d_to, core, sub], zr if to_right else zl)

    zr_a, zl_b = key_send(0, s0, True), key_send(0, s1, False)
    zr_b, zl_a = key_send(0, s1, True), key_send(0, s0, False)

    rounded = lambda k: (a5[:, 128 * k : 128 * (k + 1)] * scale).astype(BF16).astype(F32)
    cprod[...] = (rounded(1) * rounded(0)).astype(BF16)
    to_next = remote(cprod.at[pl.ds(T - 16, 16)], halo.at[0], span_next)
    to_prev = remote(cprod.at[pl.ds(0, 16)], halo.at[1], span_prev)

    q_scale = scale_row * ((NOPE + ROPE) ** (-0.5) * math.log2(math.e))
    for h in range(2):
        qs[0, h, pl.ds(0, NOPE), :] = (aqr[pl.ds(96 * h, NOPE), :] * q_scale).astype(BF16)
        qs[0, h, pl.ds(NOPE, ROPE), :] = turned(aqr[pl.ds(96 * h + NOPE, ROPE), :] * q_scale).astype(BF16)
    q96 = pl.ds(0, 96)
    qr0 = remote(qs.at[0, 0, q96], qs.at[1, 0, q96], yr)
    ql0 = remote(qs.at[0, 1, q96], qs.at[2, 1, q96], yl)
    qr1 = remote(qs.at[0, 1, q96], qs.at[1, 1, q96], yr)
    ql1 = remote(qs.at[0, 0, q96], qs.at[2, 0, q96], yl)

    w0, w1 = pl.ds(0, 64), pl.ds(64, 64)
    wr0 = remote(wall.at[0, 0, w0], wall.at[1, 0, w0], xr)
    wl0 = remote(wall.at[0, 0, w1], wall.at[2, 0, w1], xl)
    wr1 = remote(wall.at[0, 0, w1], wall.at[1, 0, w1], xr)
    wl1 = remote(wall.at[0, 0, w0], wall.at[2, 0, w0], xl)
    wd0 = remote(wall.at[0, 0], wall.at[0, 1], partner)

    ku2[...] = mm(
        ku_raw[...], selection(128, 256, lambda r, c: (c % 128 < 64) & (r == c // 128 * 64 + c % 128))
    ).astype(BF16)
    vu_t = jnp.transpose(vu_raw[...].astype(F32)).astype(BF16)
    e_k = selection(ROPE, 256, lambda r, c: (c % 128 >= 64) & (c % 128 < 96) & (r == c % 128 - 64))
    place = {d: n * T for n, d in enumerate(ARRIVAL)}

    def build(d):
        piece = jnp.concatenate([msg[d, 0], msg[d, 1]], axis=0)
        lat = piece[:T]
        for g in range(2):
            pk = jnp.transpose(piece[T + ROPE * g : T + ROPE * (g + 1)].astype(F32)).astype(BF16)
            k = mm(lat[256 * g : 256 * (g + 1)], ku2[...]) + mm(pk, e_k)
            kall[pl.ds(place[d] + 256 * g, 256), :] = k.astype(BF16)
        v = lax.dot_general(vu_t, lat, (((1,), (1,)), ((), ())), preferred_element_type=F32).astype(BF16)
        for h in range(2):
            vt[h, pl.ds(0, VDIM), pl.ds(place[d], T)] = v[VDIM * h : VDIM * (h + 1)]

    build(0)

    right_a, left_b, right_b, left_a, swaps = {0: zr_a}, {0: zl_b}, {0: zr_b}, {0: zl_a}, {}

    def step_a(step):
        right_a[step - 1].wait_recv()
        if step < 4:
            right_a[step] = key_send(step, s0, True)
        left_b[step - 1].wait_recv()
        if step < 4:
            left_b[step] = key_send(step, s1, False)
        else:
            swaps[4] = remote(msg.at[4, core], msg.at[4, core], partner)

    def step_b(step):
        right_b[step - 1].wait_recv()
        if step < 3:
            right_b[step] = key_send(step, s1, True)
        left_a[step - 1].wait_recv()
        if step < 3:
            left_a[step] = key_send(step, s0, False)
        for d in (step, NZ - step):
            swaps[d] = remote(msg.at[d, core], msg.at[d, core], partner)

    def arrive(*pieces):
        for d in pieces:
            swaps[d].wait_recv()
            build(d)

    groups = ((0, 3), (3, 2), (5, 3))

    def stage(new, old, top_old):
        top_new = None
        if new is not None:
            (first, count), i, h = groups[new[0]], new[1], new[2]
            mx = None
            for j in range(count * T // CHUNK):
                s = mm(kall[pl.ds(first * T + j * CHUNK, CHUNK), 128 * h : 128 * (h + 1)], qs[i, h])
                sbuf[h, pl.ds(j * CHUNK, CHUNK), :] = s
                m = jnp.max(s.reshape(CHUNK // 8, 8, T), axis=0)
                mx = m if mx is None else jnp.maximum(mx, m)
            top_new = jnp.max(mx, axis=0, keepdims=True)
        if old is not None:
            (first, count), i, h = groups[old[0]], old[1], old[2]
            if old[0] > 0:
                before = tops[i, h, pl.ds(0, 1), :]
                top_old = jnp.maximum(before, top_old)
            total = None
            for j in range(count * T // CHUNK):
                p = jnp.exp2(sbuf[h, pl.ds(j * CHUNK, CHUNK), :] - top_old).astype(BF16)
                term = mm(vt[h, :, pl.ds(first * T + j * CHUNK, CHUNK)], p)
                total = term if total is None else total + term
            if old[0] > 0:
                total = total + acc[i, h] * jnp.exp2(before - top_old)
            acc[i, h] = total
            tops[i, h] = jnp.broadcast_to(top_old, (8, T))
        return top_new

    def finish(i, h):
        total = acc[i, h, pl.ds(VDIM, 1), :]
        om[i, h] = (acc[i, h, pl.ds(0, VDIM), :] * (1.0 / total)).astype(BF16)
        ostat[i, h] = jnp.concatenate([tops[i, h, pl.ds(0, 1), :], total], axis=0)

    def merged(parts):
        parts = [(o[...].astype(F32), st[...]) for o, st in parts]
        top = parts[0][1][0:1]
        for _, st in parts[1:]:
            top = jnp.maximum(top, st[0:1])
        weights = [st[1:2] * jnp.exp2(st[0:1] - top) for _, st in parts]
        total, summed = weights[0], parts[0][0] * weights[0]
        for w, (o, _) in zip(weights[1:], parts[1:]):
            total, summed = total + w, summed + o * w
        return summed / total, jnp.concatenate([top, total], axis=0)

    lo, hi = slice(0, 1024), slice(1024, 2048)
    order = (2, 1, 3, 0)
    sums = {}

    def conv_rows(r, c):
        return conv_out[pl.ds(pl.multiple_of((x + r) % NX * 128 + c * 64, 64), 64), :]

    def conv_partials():
        for r in order:
            p_send[r] = mm(conv_rows(r, other), wd[...]).astype(BF16)
            sums[r] = remote(p_send.at[r], p_recv.at[r], partner)
        for r in order:
            own[r] = mm(conv_rows(r, core), wd[...])

    def conv_first():
        sums[2].wait_recv()
        for k, cols in enumerate((lo, hi)):
            pair2[k] = (own[2, :, cols] + p_recv[2, :, cols].astype(F32)).astype(BF16)
        sums["a"] = remote(pair2.at[0], turn_a, xr)
        sums["b"] = remote(pair2.at[1], turn_b, xl)
        sums[1].wait_recv()
        pair1[1] = (own[1, :, hi] + p_recv[1, :, hi].astype(F32)).astype(BF16)
        sums["far_r"] = remote(pair1.at[1], from_l.at[1], xr)
        sums[3].wait_recv()
        pair3[0] = (own[3, :, lo] + p_recv[3, :, lo].astype(F32)).astype(BF16)
        sums["far_l"] = remote(pair3.at[0], from_r.at[0], xl)

    def conv_second():
        sums["a"].wait_recv()
        pair1[0] = (own[1, :, lo] + p_recv[1, :, lo].astype(F32) + turn_a[...].astype(F32)).astype(BF16)
        sums["near_r"] = remote(pair1.at[0], from_l.at[0], xr)
        sums["b"].wait_recv()
        pair3[1] = (own[3, :, hi] + p_recv[3, :, hi].astype(F32) + turn_b[...].astype(F32)).astype(BF16)
        sums["near_l"] = remote(pair3.at[1], from_r.at[1], xl)

    weight_hops = {}

    def weights_on(k):
        if k == 0:
            wr0.wait_recv()
            weight_hops["r"] = remote(wall.at[1, 0, w0], wall.at[3, 0, w0], xr)
            wl0.wait_recv()
            weight_hops["l"] = remote(wall.at[2, 0, w1], wall.at[3, 0, w1], xl)
        elif k == 1:
            wr1.wait_recv()
            weight_hops[1] = remote(wall.at[1, 0], wall.at[1, 1], partner)
            wl1.wait_recv()
            weight_hops[2] = remote(wall.at[2, 0], wall.at[2, 1], partner)
        else:
            weight_hops["r"].wait_recv()
            weight_hops["l"].wait_recv()
            weight_hops[3] = remote(wall.at[3, 0], wall.at[3, 1], partner)

    step_a(1)
    step_b(1)
    qr0.wait_recv()
    qr2 = remote(qs.at[1, 0, q96], qs.at[3, 0, q96], yr)
    ql0.wait_recv()
    ql2 = remote(qs.at[2, 1, q96], qs.at[3, 1, q96], yl)
    to_next.wait_recv()
    to_prev.wait_recv()
    cp = cprod[...].astype(F32)
    row = iota((T, 128), 0)
    before = jnp.where(sp > 0, halo[0].astype(F32)[15:16], 0.0)
    after = jnp.where(sp < NY * NZ - 1, halo[1].astype(F32)[0:1], 0.0)
    tap = taps[...].astype(F32)
    mixed = (
        jnp.where(row == 0, before, pltpu.roll(cp, 1, 0)) * tap[0:1]
        + cp * tap[1:2]
        + jnp.where(row == T - 1, after, pltpu.roll(cp, T - 1, 0)) * tap[2:3]
    )
    conv_out[...] = (silu(rounded(3)) * rounded(2) * mixed).astype(BF16)
    gate_out[...] = silu(rounded(4))
    arrive(1, 7)

    def key_events(n):
        if n == 0:
            step_a(2)
        elif n == 1:
            weights_on(0)
        elif n == 2:
            qr1.wait_recv()
            ql1.wait_recv()
        elif n == 3:
            step_b(2)
        elif n == 5:
            step_a(3)
            qr2.wait_recv()
            ql2.wait_recv()
        elif n == 7:
            arrive(2, 6)
        elif n == 8:
            step_b(3)
            weights_on(1)
        elif n == 9:
            conv_partials()
        elif n == 12:
            step_a(4)
            conv_first()
        elif n == 13:
            arrive(3, 5, 4)
        elif n == 16:
            weights_on(2)
        elif n == 19:
            conv_second()

    units = [(0, i, h) for i in (0, 1, 2, 3) for h in range(2)]
    units += [(g, i, h) for g in (1, 2) for i in (3, 2, 1) for h in range(2)]
    units += [(g, 0, h) for g in (1, 2) for h in range(2)]
    back = {}
    top = stage(units[0], None, None)
    for n, (group, i, h) in enumerate(units):
        key_events(n)
        unit = (i, h)
        top = stage(units[n + 1] if n + 1 < len(units) else None, units[n], top)
        if group < 2:
            continue
        finish(i, h)
        if i == 3:
            to = yr if h == 0 else yl
            back[unit] = (remote(om.at[i, h], relay.at[h], to), remote(ostat.at[i, h], relay_stat.at[h], to))
        elif unit == (2, 1):
            back["l", 1] = (remote(om.at[2, 1], ro.at[0, 1], yr), remote(ostat.at[2, 1], rstat.at[0, 1], yr))
        elif unit == (1, 0):
            back["r", 0] = (remote(om.at[1, 0], ro.at[1, 0], yl), remote(ostat.at[1, 0], rstat.at[1, 0], yl))
        elif unit == (1, 1):
            for k, i2, to, side in ((0, 2, yr, "l"), (1, 1, yl, "r")):
                for c in back[(3, k)]:
                    c.wait_recv()
                o, st = merged([(om.at[i2, k], ostat.at[i2, k]), (relay.at[k], relay_stat.at[k])])
                both[k] = o.astype(BF16)
                both_stat[k] = st
                slot = 0 if side == "l" else 1
                back[side, k] = (
                    remote(both.at[k], ro.at[slot, k], to), remote(both_stat.at[k], rstat.at[slot, k], to)
                )
    for side in "lr":
        for k in range(2):
            for c in back[side, k]:
                c.wait_recv()
    parts = [
        merged([(om.at[0, h], ostat.at[0, h])] + [(ro.at[k, h], rstat.at[k, h]) for k in range(2)])[0]
        for h in range(2)
    ]
    attended = jnp.transpose(jnp.concatenate(parts, axis=0))
    aout[...] = (gate_out[...] * attended).astype(BF16)

    def tile(r, c):
        return aout.at[pl.ds(pl.multiple_of((x + r) % NX * 128 + c * 64, 64), 64)]

    tiles = []
    for r, slot in ((2, 3), (1, 1), (3, 2), (0, 0)):
        for k, c in enumerate((core, other)):
            if r or k:
                tiles.append(remote(tile(r, c), aall.at[slot, k], tp_peer(r, c) if r else partner))
    aall[0, 0] = tile(0, core)[...]
    for k in (0, "far_r", "far_l", "near_r", "near_l"):
        sums[k].wait_recv()
    for k, cols in enumerate((lo, hi)):
        own[0, :, cols] = (
            own[0, :, cols] + p_recv[0, :, cols].astype(F32) + from_l[k].astype(F32) + from_r[k].astype(F32)
        )
    wd0.wait_recv()
    for k in (1, 2, 3):
        weight_hops[k].wait_recv()
    for c in tiles:
        c.wait_recv()
    rows = jnp.concatenate([aall[s, k] for s in range(NX) for k in range(2)], axis=1)
    for n in range(4):
        cols = pl.ds(512 * n, 512)
        term = own[0, :, cols]
        for s in range(NX):
            w = jnp.concatenate([wall[s, 0, :, cols], wall[s, 1, :, cols]], axis=0)
            term = term + mm(rows[:, 256 * s : 256 * (s + 1)], w)
        out[:, cols] = term.astype(BF16)
    for c in started:
        c.wait_send()


def scratch():
    v = lambda shape, kind=BF16: pltpu.VMEM(shape, kind)
    return [
        v((8, T, FB)), v((D, 640)), v((224, D)), v((D, 256)),
        v((256, 128)), v((256, 256)), v((256, 128)), v((128, D)), v((3, 128)), v((256,), F32),
        v((T, 640), F32), v((T, 256), F32), v((224, T), F32), v((T, 128), F32),
        v((NZ, 2, HALF, 256)), v((NY, 2, 128, T)), v((KEYS, 256)), v((2, VROWS, KEYS)),
        v((2, 3 * T, T), F32), v((NY, 2, VROWS, T), F32), v((NY, 2, 8, T), F32),
        v((NY, 2, VDIM, T)), v((NY, 2, 2, T), F32), v((2, 2, VDIM, T)), v((2, 2, 2, T), F32),
        v((2, VDIM, T)), v((2, 2, T), F32), v((2, VDIM, T)), v((2, 2, T), F32),
        v((NX, 2, 128, D)), v((T, 128)), v((NX, 2, 64, 128)),
        v((T, 128)), v((2, 16, 128)), v((T, 128)), v((T, 128), F32),
        v((NX, 64, D)), v((NX, 64, D)), v((NX, 64, D), F32),
        v((2, 64, 1024)), v((2, 64, 1024)), v((2, 64, 1024)), v((64, 1024)), v((64, 1024)),
        v((2, 64, 1024)), v((2, 64, 1024)),
        pltpu.SemaphoreType.DMA((N_REMOTE,)), pltpu.SemaphoreType.DMA((N_REMOTE,)),
        pltpu.SemaphoreType.DMA((N_LOCAL,)),
    ]


def on_device(*args):
    args = tuple(a.T if k in (6, 8) else a for k, a in enumerate(args))
    return pl.pallas_call(
        layer_kernel,
        out_shape=jax.ShapeDtypeStruct((64, D), BF16),
        in_specs=[pl.BlockSpec(memory_space=pl.ANY)] * len(args),
        out_specs=pl.BlockSpec(memory_space=pltpu.VMEM),
        scratch_shapes=scratch(),
        compiler_params=pltpu.CompilerParams(
            collective_id=0, has_side_effects=True, vmem_limit_bytes=62 * 1024 * 1024
        ),
        name="layer",
    )(*args)


def solution(mesh):
    cols, rows, whole = P(None, "tp"), P("tp", None), P()
    placed = (P("sp", "tp"), cols, cols, cols, cols, cols, cols, whole, whole, whole, cols, cols, cols, rows, rows)
    return jax.shard_map(
        on_device, mesh=mesh, in_specs=placed, out_specs=P(("sp", "tp"), None), check_vma=False
    )
```

time: 87.1 us -> 66.1 us (0.76)
  Pallas kernels: 81.2 us -> 64.3 us
  local copies, waits for them, and re-layouts: 5.83 us -> 1.67 us
    pallas_call x1, Pallas kernels: 81.2 us -> 64.3 us  [on_device(): pl.pallas_call(layer_kernel, out_shape=jax.ShapeDtypeStruct((64, D), BF16...]
    unnamed x3 -> x1, local copies, waits for them, and re-layouts: 5.83 us -> 1.67 us
where the time goes in v2:
time: 66.1 us; the launch traced here: 66 us
  Pallas kernels  64.3 us (97%)
  local copies, waits for them, and re-layouts  1.67 us (3%)
    pallas_call x1, Pallas kernels, on_device(): pl.pallas_call(layer_kernel, out_shape=jax.ShapeDtypeStruct((64, D), BF16...  64.3 us
    unnamed x1, local copies, waits for them, and re-layouts  1.67 us

profile of v2, /device:TPU:1, one launch (start us, length us, event | category | flops | bytes accessed | tf_op | source)
XLA Modules:
  0.0 66.0 jit_solution(7450898750921521301)
XLA Ops:
  0.0 64.3 %layer.1 = bf16[64,2048]{1,0:T(8,128)(2,1)} custom-call(bf16[512,256]{1,0:T(8,128)(2,1)} %tokens.1, bf16[2048,128]{1,0:T(8,128)(2,1)} %conv_input.1, bf16[2048,128]{1,0:T(8,128)(2,1)} %conv_inner.1, bf16[2048,128]{1,0:T(8,128)(2,1)} %conv_outer.1, bf16[2048,128]{1,0:T(8,128)(2,1)} %conv_gate.1, bf16[3,128]{1,0:T(4,128)(2,1)} %conv_taps.1, ...), custom_call_target="tpu_custom_call" | custom-call | tf_op jit(solution)/shard_map/layer/pallas_call | solution.py:522
  64.3 1.7 %copy.17 = bf16[64,2048]{1,0:T(8,128)(2,1)} copy(bf16[64,2048]{1,0:T(8,128)(2,1)} %layer.1) | data formatting | bytes 524288

commit v3 on v2

--- a/solution.py
+++ b/solution.py
@@ -19,7 +19,7 @@
 HALF = PIECE // 2
 SUB = HALF // 2
 VROWS = VDIM + 16
-CHUNK = 512
+CHUNK = 256
 ARRIVAL = (0, 1, 7, 2, 6, 3, 5, 4)
 N_REMOTE = 96
 N_LOCAL = 16
@@ -47,7 +47,7 @@
     tokens, conv_input, conv_inner, conv_outer, conv_gate, conv_taps, query_proj, latent_proj,
     rope_proj, latent_gain, key_up, value_up, attn_gate, conv_down, attn_down,
     out,
-    xall, w5, wqr, wl, ku_raw, ku2, vu_raw, wd, taps, gain,
+    xall, w5, wqr, wl, ku_raw, ku2, vu_raw, vu_t, e_k, wd, taps, gain,
     a5, al, aqr, ss,
     msg, qs, kall, vt, sbuf, acc, tops,
     om, ostat, ro, rstat, relay, relay_stat, both, both_stat,
@@ -92,7 +92,8 @@
         for k, w in enumerate((conv_input, conv_inner, conv_outer, conv_gate, attn_gate))
     ]
     loads_proj.append(load(latent_proj, wl))
-    loads_late = [load(conv_taps, taps), load(latent_gain, gain), load(key_up, ku_raw), load(value_up, vu_raw)]
+    loads_late = [load(conv_taps, taps), load(latent_gain, gain)]
+    loads_kv = [load(key_up, ku_raw), load(value_up, vu_raw)]
     loads_late += [load(conv_down, wd), load(attn_down, wall.at[0, 0])]
 
     barrier = pltpu.get_barrier_semaphore()
@@ -127,22 +128,24 @@
     for c in loads_proj:
         c.wait()
 
-    def project(slot, chip, c, first=False):
+    def project(slot, chip, c, first=False, early=True, late=True):
         block = pl.multiple_of((chip * 2 + c) * FB, FB)
 
         def rows_of(i, _):
             rows = pl.ds(pl.multiple_of(i * 256, 256), 256)
             v = xall[slot, rows, :]
-            wide = v.astype(F32)
-            squares = wide[:, :128] * wide[:, :128] + wide[:, 128:] * wide[:, 128:]
-            for total, w in ((a5, w5), (al, wl)):
-                term = mm(v, w[pl.ds(block, FB), :])
-                total[rows, :] = term if first else total[rows, :] + term
-            term = lax.dot_general(
-                wqr[:, pl.ds(block, FB)], v, (((1,), (1,)), ((), ())), preferred_element_type=F32
-            )
-            aqr[:, rows] = term if first else aqr[:, rows] + term
-            ss[rows, :] = squares if first else ss[rows, :] + squares
+            if early:
+                wide = v.astype(F32)
+                squares = wide[:, :128] * wide[:, :128] + wide[:, 128:] * wide[:, 128:]
+                ss[rows, :] = squares if first else ss[rows, :] + squares
+                term = lax.dot_general(
+                    wqr[:, pl.ds(block, FB)], v, (((1,), (1,)), ((), ())), preferred_element_type=F32
+                )
+                aqr[:, rows] = term if first else aqr[:, rows] + term
+            for total, w, now in ((al, wl, early), (a5, w5, late)):
+                if now:
+                    term = mm(v, w[pl.ds(block, FB), :])
+                    total[rows, :] = term if first else total[rows, :] + term
             return 0
 
         lax.fori_loop(0, T // 256, rows_of, 0)
@@ -155,6 +158,13 @@
     project(0, x, core, first=True)
     d0.wait_recv()
     project(4, x, other)
+    for c in loads_kv:
+        c.wait()
+    ku2[...] = mm(
+        ku_raw[...], selection(128, 256, lambda r, c: (c % 128 < 64) & (r == c // 128 * 64 + c % 128))
+    ).astype(BF16)
+    vu_t[...] = jnp.transpose(vu_raw[...].astype(F32)).astype(BF16)
+    e_k[...] = selection(ROPE, 256, lambda r, c: (c % 128 >= 64) & (c % 128 < 96) & (r == c % 128 - 64))
     r1.wait_recv()
     d1 = remote(xall.at[1], xall.at[5], partner)
     l1.wait_recv()
@@ -168,11 +178,11 @@
     l2.wait_recv()
     d3b = remote(xall.at[3, h1], xall.at[7, h1], partner)
     d2.wait_recv()
-    project(6, right, other)
-    project(3, across, core)
+    project(6, right, other, late=False)
+    project(3, across, core, late=False)
     d3a.wait_recv()
     d3b.wait_recv()
-    project(7, across, other)
+    project(7, across, other, late=False)
     for c in loads_late:
         c.wait()
 
@@ -203,11 +213,6 @@
 
     zr_a, zl_b = key_send(0, s0, True), key_send(0, s1, False)
     zr_b, zl_a = key_send(0, s1, True), key_send(0, s0, False)
-
-    rounded = lambda k: (a5[:, 128 * k : 128 * (k + 1)] * scale).astype(BF16).astype(F32)
-    cprod[...] = (rounded(1) * rounded(0)).astype(BF16)
-    to_next = remote(cprod.at[pl.ds(T - 16, 16)], halo.at[0], span_next)
-    to_prev = remote(cprod.at[pl.ds(0, 16)], halo.at[1], span_prev)
 
     q_scale = scale_row * ((NOPE + ROPE) ** (-0.5) * math.log2(math.e))
     for h in range(2):
@@ -226,11 +231,6 @@
     wl1 = remote(wall.at[0, 0, w0], wall.at[2, 0, w0], xl)
     wd0 = remote(wall.at[0, 0], wall.at[0, 1], partner)
 
-    ku2[...] = mm(
-        ku_raw[...], selection(128, 256, lambda r, c: (c % 128 < 64) & (r == c // 128 * 64 + c % 128))
-    ).astype(BF16)
-    vu_t = jnp.transpose(vu_raw[...].astype(F32)).astype(BF16)
-    e_k = selection(ROPE, 256, lambda r, c: (c % 128 >= 64) & (c % 128 < 96) & (r == c % 128 - 64))
     place = {d: n * T for n, d in enumerate(ARRIVAL)}
 
     def build(d):
@@ -238,13 +238,21 @@
         lat = piece[:T]
         for g in range(2):
             pk = jnp.transpose(piece[T + ROPE * g : T + ROPE * (g + 1)].astype(F32)).astype(BF16)
-            k = mm(lat[256 * g : 256 * (g + 1)], ku2[...]) + mm(pk, e_k)
+            k = mm(lat[256 * g : 256 * (g + 1)], ku2[...]) + mm(pk, e_k[...])
             kall[pl.ds(place[d] + 256 * g, 256), :] = k.astype(BF16)
-        v = lax.dot_general(vu_t, lat, (((1,), (1,)), ((), ())), preferred_element_type=F32).astype(BF16)
+        v = lax.dot_general(vu_t[...], lat, (((1,), (1,)), ((), ())), preferred_element_type=F32).astype(BF16)
         for h in range(2):
             vt[h, pl.ds(0, VDIM), pl.ds(place[d], T)] = v[VDIM * h : VDIM * (h + 1)]
 
     build(0)
+
+    project(6, right, other, early=False)
+    project(3, across, core, early=False)
+    project(7, across, other, early=False)
+    rounded = lambda k: (a5[:, 128 * k : 128 * (k + 1)] * scale).astype(BF16).astype(F32)
+    cprod[...] = (rounded(1) * rounded(0)).astype(BF16)
+    to_next = remote(cprod.at[pl.ds(T - 16, 16)], halo.at[0], span_next)
+    to_prev = remote(cprod.at[pl.ds(0, 16)], halo.at[1], span_prev)
 
     right_a, left_b, right_b, left_a, swaps = {0: zr_a}, {0: zl_b}, {0: zr_b}, {0: zl_a}, {}
 
@@ -271,6 +279,7 @@
     def arrive(*pieces):
         for d in pieces:
             swaps[d].wait_recv()
+        for d in pieces:
             build(d)
 
     groups = ((0, 3), (3, 2), (5, 3))
@@ -322,15 +331,24 @@
     order = (2, 1, 3, 0)
     sums = {}
 
-    def conv_rows(r, c):
-        return conv_out[pl.ds(pl.multiple_of((x + r) % NX * 128 + c * 64, 64), 64), :]
+    def conv_rows(c):
+        at = lambda r: pl.ds(pl.multiple_of((x + r) % NX * 128 + c * 64, 64), 64)
+        return jnp.concatenate([conv_out[at(r), :] for r in range(NX)], axis=0)
 
     def conv_partials():
+        theirs, ours = conv_rows(other), conv_rows(core)
+        for n in range(4):
+            cols = slice(512 * n, 512 * (n + 1))
+            term = mm(theirs, wd[:, cols]).astype(BF16)
+            for r in range(NX):
+                p_send[r, :, cols] = term[64 * r : 64 * (r + 1)]
         for r in order:
-            p_send[r] = mm(conv_rows(r, other), wd[...]).astype(BF16)
             sums[r] = remote(p_send.at[r], p_recv.at[r], partner)
-        for r in order:
-            own[r] = mm(conv_rows(r, core), wd[...])
+        for n in range(4):
+            cols = slice(512 * n, 512 * (n + 1))
+            term = mm(ours, wd[:, cols])
+            for r in range(NX):
+                own[r, :, cols] = term[64 * r : 64 * (r + 1)]
 
     def conv_first():
         sums[2].wait_recv()
@@ -391,6 +409,7 @@
     )
     conv_out[...] = (silu(rounded(3)) * rounded(2) * mixed).astype(BF16)
     gate_out[...] = silu(rounded(4))
+    conv_partials()
     arrive(1, 7)
 
     def key_events(n):
@@ -412,11 +431,10 @@
         elif n == 8:
             step_b(3)
             weights_on(1)
-        elif n == 9:
-            conv_partials()
+        elif n == 10:
+            conv_first()
         elif n == 12:
             step_a(4)
-            conv_first()
         elif n == 13:
             arrive(3, 5, 4)
         elif n == 16:
@@ -468,11 +486,11 @@
     def tile(r, c):
         return aout.at[pl.ds(pl.multiple_of((x + r) % NX * 128 + c * 64, 64), 64)]
 
-    tiles = []
+    tiles = {}
     for r, slot in ((2, 3), (1, 1), (3, 2), (0, 0)):
         for k, c in enumerate((core, other)):
             if r or k:
-                tiles.append(remote(tile(r, c), aall.at[slot, k], tp_peer(r, c) if r else partner))
+                tiles[slot, k] = remote(tile(r, c), aall.at[slot, k], tp_peer(r, c) if r else partner)
     aall[0, 0] = tile(0, core)[...]
     for k in (0, "far_r", "far_l", "near_r", "near_l"):
         sums[k].wait_recv()
@@ -483,16 +501,19 @@
     wd0.wait_recv()
     for k in (1, 2, 3):
         weight_hops[k].wait_recv()
-    for c in tiles:
-        c.wait_recv()
-    rows = jnp.concatenate([aall[s, k] for s in range(NX) for k in range(2)], axis=1)
-    for n in range(4):
-        cols = pl.ds(512 * n, 512)
-        term = own[0, :, cols]
-        for s in range(NX):
-            w = jnp.concatenate([wall[s, 0, :, cols], wall[s, 1, :, cols]], axis=0)
-            term = term + mm(rows[:, 256 * s : 256 * (s + 1)], w)
-        out[:, cols] = term.astype(BF16)
+    for slot in range(NX):
+        for k in range(2):
+            if slot or k:
+                tiles[slot, k].wait_recv()
+        rows = jnp.concatenate([aall[slot, 0], aall[slot, 1]], axis=1)
+        for n in range(4):
+            cols = pl.ds(512 * n, 512)
+            w = jnp.concatenate([wall[slot, 0, :, cols], wall[slot, 1, :, cols]], axis=0)
+            term = own[0, :, cols] + mm(rows, w)
+            if slot < NX - 1:
+                own[0, :, cols] = term
+            else:
+                out[:, cols] = term.astype(BF16)
     for c in started:
         c.wait_send()
 
@@ -501,7 +522,7 @@
     v = lambda shape, kind=BF16: pltpu.VMEM(shape, kind)
     return [
         v((8, T, FB)), v((D, 640)), v((224, D)), v((D, 256)),
-        v((256, 128)), v((256, 256)), v((256, 128)), v((128, D)), v((3, 128)), v((256,), F32),
+        v((256, 128)), v((256, 256)), v((256, 128)), v((128, 256)), v((ROPE, 256)), v((128, D)), v((3, 128)), v((256,), F32),
         v((T, 640), F32), v((T, 256), F32), v((224, T), F32), v((T, 128), F32),
         v((NZ, 2, HALF, 256)), v((NY, 2, 128, T)), v((KEYS, 256)), v((2, VROWS, KEYS)),
         v((2, 3 * T, T), F32), v((NY, 2, VROWS, T), F32), v((NY, 2, 8, T), F32),

time: 66.1 us -> 64.6 us (0.977)
  Pallas kernels: 64.3 us -> 62.8 us
    pallas_call x1, Pallas kernels: 64.3 us -> 62.8 us  [on_device(): pl.pallas_call(layer_kernel, out_shape=jax.ShapeDtypeStruct((64, D), BF16...]
where the time goes in v3:
time: 64.6 us; the launch traced here: 64.5 us
  Pallas kernels  62.8 us (97%)
  local copies, waits for them, and re-layouts  1.67 us (3%)
    pallas_call x1, Pallas kernels, on_device(): pl.pallas_call(layer_kernel, out_shape=jax.ShapeDtypeStruct((64, D), BF16...  62.8 us
    unnamed x1, local copies, waits for them, and re-layouts  1.67 us

profile of v3, /device:TPU:1, one launch (start us, length us, event | category | flops | bytes accessed | tf_op | source)
XLA Modules:
  0.0 64.5 jit_solution(13819793829198490975)
XLA Ops:
  0.0 62.8 %layer.1 = bf16[64,2048]{1,0:T(8,128)(2,1)} custom-call(bf16[512,256]{1,0:T(8,128)(2,1)} %tokens.1, bf16[2048,128]{1,0:T(8,128)(2,1)} %conv_input.1, bf16[2048,128]{1,0:T(8,128)(2,1)} %conv_inner.1, bf16[2048,128]{1,0:T(8,128)(2,1)} %conv_outer.1, bf16[2048,128]{1,0:T(8,128)(2,1)} %conv_gate.1, bf16[3,128]{1,0:T(4,128)(2,1)} %conv_taps.1, ...), custom_call_target="tpu_custom_call" | custom-call | tf_op jit(solution)/shard_map/layer/pallas_call | solution.py:543
  62.8 1.7 %copy.17 = bf16[64,2048]{1,0:T(8,128)(2,1)} copy(bf16[64,2048]{1,0:T(8,128)(2,1)} %layer.1) | data formatting | bytes 524288

commit v4 on v3

--- a/solution.py
+++ b/solution.py
@@ -98,8 +98,7 @@
 
     barrier = pltpu.get_barrier_semaphore()
     tp_peer = lambda r, c: dev(sp, (x + r) % NX * 2 + c)
-    peers = [tp_peer(r, c) for r in (1, 2, 3) for c in (core, other)]
-    peers += [partner, yr, yl, zr, zl, span_next, span_prev]
+    peers = [partner, xr, xl, yr, yl, zr, zl, span_next, span_prev]
     for to in peers:
         pl.semaphore_signal(barrier, inc=1, device_id=to, device_id_type=MESH)
     pl.semaphore_wait(barrier, len(peers))

time: 64.6 us -> 64.5 us (level)
  no operation moved by 1% of the time
where the time goes in v4:
time: 64.5 us; the launch traced here: 64.4 us
  Pallas kernels  62.8 us (97%)
  local copies, waits for them, and re-layouts  1.67 us (3%)
    pallas_call x1, Pallas kernels, on_device(): pl.pallas_call(layer_kernel, out_shape=jax.ShapeDtypeStruct((64, D), BF16...  62.8 us
    unnamed x1, local copies, waits for them, and re-layouts  1.67 us

profile of v4, /device:TPU:1, one launch (start us, length us, event | category | flops | bytes accessed | tf_op | source)
XLA Modules:
  0.0 64.4 jit_solution(11733139458794064851)
XLA Ops:
  0.0 62.8 %layer.1 = bf16[64,2048]{1,0:T(8,128)(2,1)} custom-call(bf16[512,256]{1,0:T(8,128)(2,1)} %tokens.1, bf16[2048,128]{1,0:T(8,128)(2,1)} %conv_input.1, bf16[2048,128]{1,0:T(8,128)(2,1)} %conv_inner.1, bf16[2048,128]{1,0:T(8,128)(2,1)} %conv_outer.1, bf16[2048,128]{1,0:T(8,128)(2,1)} %conv_gate.1, bf16[3,128]{1,0:T(4,128)(2,1)} %conv_taps.1, ...), custom_call_target="tpu_custom_call" | custom-call | tf_op jit(solution)/shard_map/layer/pallas_call | solution.py:542
  62.8 1.7 %copy.17 = bf16[64,2048]{1,0:T(8,128)(2,1)} copy(bf16[64,2048]{1,0:T(8,128)(2,1)} %layer.1) | data formatting | bytes 524288
